TPU v7x, 512 devices: a whole 4x8x8 slice. The times are simulated.
512 devices in a mesh: sp: 64 (over z, y), tp: 8 (over x, core).
Axes of the slice: x: 4, y: 8, z: 8, core: 2. Of those that a mesh axis runs over, the one named last changes fastest.
Arguments:
- tokens: bfloat16 [65536, 2048], P(('sp', 'tp')), may hold values from -6 to 6
- norm_gain: float32 [2048], replicated, may hold values from 0.1 to 1.9
- w_query: bfloat16 [2048, 2048], P('sp', 'tp'), may hold values from -0.125 to 0.125
- w_key: bfloat16 [2048, 2048], P('sp', 'tp'), may hold values from -0.125 to 0.125
- w_value: bfloat16 [2048, 4096], P('sp', 'tp'), may hold values from -0.125 to 0.125
- w_rank_down: bfloat16 [2048, 16], replicated, may hold values from -0.125 to 0.125
- w_rank_up: bfloat16 [16, 2048], P(None, 'tp'), may hold values from -1.5 to 1.5
- gate_bias: float32 [2048], P('tp')
- decay_shift: float32 [65536], P('sp'), may hold values from -1 to 0
- out_gain: float32 [512], replicated, may hold values from 0.1 to 1.9
- w_out: bfloat16 [4096, 2048], P('tp', 'sp'), may hold values from -0.09375 to 0.09375
Outputs:
- mixed: bfloat16 [65536, 2048], P(('sp', 'tp'))
All inputs are finite; a program needn't handle non-finite values.
Results may differ from a plain program's by a relative error of at most 0.015.
Values may be sent and summed in bfloat16 or wider, within the bound.
A program may use at most 128 MiB of HBM per device.

v0:
```python
import jax
import jax.numpy as jnp
from jax import lax
from jax.sharding import Mesh
from jax.sharding import PartitionSpec as P

DK = 256
DV = 512
TAU = 16
BLOCK = 64
SP = ("sp_0", "sp_1")
SP_TP = ("sp_0", "sp_1", "tp")
EPS = 1e-06


def sent_together(arrays, axis, dim, along):
    both = jnp.concatenate(arrays, axis=along)
    out, at, finished = (lax.all_gather(both, axis, axis=dim, tiled=True), 0, [])
    for a in arrays:
        finished.append(lax.slice_in_dim(out, at, at + a.shape[along], axis=along))
        at += a.shape[along]
    return tuple(finished)


def filled_with(value, identity):
    return jax.tree.map(
        lambda a, e: jnp.broadcast_to(jnp.asarray(e, a.dtype), a.shape), value, identity
    )


def entering(value, axes, combine, identity):
    before = start = filled_with(value, identity)
    total = value
    for axis in reversed(axes):
        size, mine = (lax.axis_size(axis), lax.axis_index(axis))
        pieces = jax.tree.map(lambda part: lax.all_gather(part, axis), total)
        inside, total = (start, start)
        for k in range(size):
            passed = k < mine
            total = combine(total, jax.tree.map(lambda part: part[k], pieces))
            inside = jax.tree.map(lambda new, old: jnp.where(passed, new, old), total, inside)
        before = combine(inside, before)
    return before


def cut_along(value, dim, size):
    before, after = (value.shape[:dim], value.shape[dim + 1 :])
    return jnp.moveaxis(value.reshape(*before, size, -1, *after), dim, 0)


def sent_and_summed(value, axis, dim):
    size = lax.axis_size(axis)
    parts = lax.all_to_all(cut_along(value, dim, size), axis, 0, 0, tiled=True)
    return jnp.sum(parts.astype(jnp.float32), axis=0)


def rms_rows(values, gain):
    wide = values.astype(jnp.float32)
    return wide * lax.rsqrt(jnp.mean(wide * wide, axis=-1, keepdims=True) + EPS) * gain


def local_pass(query, key, value, log_decay, state):
    rows, heads, width = query.shape
    blocks = rows // BLOCK

    def split(tensor):
        return tensor.reshape((blocks, BLOCK) + tensor.shape[1:])

    causal = jnp.tril(jnp.ones((BLOCK, BLOCK), dtype=bool))

    def local_step(carry, inputs):
        q_blk, k_blk, v_blk, g_blk = inputs
        cumul = jnp.cumsum(g_blk, axis=0)
        centre = cumul - cumul[BLOCK // 2]
        q_scaled = (q_blk * jnp.exp(centre)).astype(jnp.bfloat16)
        k_scaled = (k_blk * jnp.exp(-centre)).astype(jnp.bfloat16)
        scores = jnp.einsum("ihd,jhd->hij", q_scaled, k_scaled, preferred_element_type=jnp.float32)
        scores = jnp.where(causal[None], scores, 0.0).astype(jnp.bfloat16)
        within = jnp.einsum("hij,jhe->ihe", scores, v_blk, preferred_element_type=jnp.float32)
        final = cumul[-1]
        decayed = (k_blk * jnp.exp(final - cumul)).astype(jnp.bfloat16)
        nxt = jnp.exp(final)[:, :, None] * carry + jnp.einsum(
            "jhd,jhe->hde", decayed, v_blk, preferred_element_type=jnp.float32
        )
        return (nxt, (within, q_blk * jnp.exp(cumul), final, carry))

    carry, (within, reach, finals, starts) = lax.scan(
        local_step, state, (split(query), split(key), split(value), split(log_decay))
    )
    return (within, reach, finals, starts, carry)


def state_only(key, value, log_decay, state):
    rows, heads, width = key.shape
    blocks = rows // BLOCK

    def split(tensor):
        return tensor.reshape((blocks, BLOCK) + tensor.shape[1:])

    def state_step(carry, inputs):
        k_blk, v_blk, g_blk = inputs
        cumul = jnp.cumsum(g_blk, axis=0)
        final = cumul[-1]
        decayed = (k_blk * jnp.exp(final - cumul)).astype(jnp.bfloat16)
        carry = jnp.exp(final)[:, :, None] * carry + jnp.einsum(
            "jhd,jhe->hde", decayed, v_blk, preferred_element_type=jnp.float32
        )
        return (carry, final)

    carry, finals = lax.scan(state_step, state, (split(key), split(value), split(log_decay)))
    return (carry, finals)


def read_out(reach, starts):
    blocks, block, heads, width = reach.shape
    result = jnp.einsum(
        "nihd,nhde->nihe",
        reach.astype(jnp.bfloat16),
        starts.astype(jnp.bfloat16),
        preferred_element_type=jnp.float32,
    )
    return result.reshape(blocks * block, heads, -1)


def combine(earlier, later):
    return (earlier[0] * later[0], later[0][:, :, None] * earlier[1] + later[1])


def on_device(
    tokens,
    norm_gain,
    w_query,
    w_key,
    w_value,
    w_rank_down,
    w_rank_up,
    gate_bias,
    decay_shift,
    out_gain,
    w_out,
):
    normed = rms_rows(tokens, norm_gain).astype(jnp.bfloat16)
    query_w, key_w, value_w = sent_together((w_query, w_key, w_value), SP, 0, 1)
    keys_here = query_w.shape[1]
    vals_here = value_w.shape[1]
    heads_here = keys_here // DK
    w_joined = jnp.concatenate([query_w, key_w, value_w, w_rank_down], axis=1)
    joined = jnp.dot(
        lax.all_gather(normed, "tp", axis=0, tiled=True),
        w_joined,
        preferred_element_type=jnp.float32,
    ).astype(jnp.bfloat16)
    span = joined.shape[0]
    q_heads = joined[:, :keys_here].astype(jnp.float32).reshape(span, heads_here, DK) * DK ** (-0.5)
    k_heads = joined[:, keys_here : 2 * keys_here].astype(jnp.float32).reshape(span, heads_here, DK)
    v_heads = joined[:, 2 * keys_here : 2 * keys_here + vals_here].reshape(span, heads_here, DV)
    rank = joined[:, 2 * keys_here + vals_here :]
    pre = jnp.dot(rank, w_rank_up, preferred_element_type=jnp.float32) + gate_bias
    log_decay = (jax.nn.log_sigmoid(pre) / TAU + decay_shift[:, None]).reshape(span, heads_here, DK)
    empty = jnp.zeros((heads_here, DK, DV), jnp.float32)
    identity = (jnp.ones((heads_here, DK), jnp.float32), empty)
    local_end, finals = state_only(k_heads, v_heads, log_decay, empty)
    carried = entering((jnp.exp(jnp.sum(finals, axis=0)), local_end), SP, combine, identity)[1]
    within, reach, _, starts, _ = local_pass(q_heads, k_heads, v_heads, log_decay, carried)
    attended = within.reshape(span, heads_here, DV) + read_out(reach, starts)
    shaped = rms_rows(attended, out_gain).astype(jnp.bfloat16).reshape(span, heads_here * DV)
    out_whole = lax.all_gather(w_out, SP, axis=1, tiled=True)
    return sent_and_summed(
        jnp.dot(shaped, out_whole, preferred_element_type=jnp.float32).astype(jnp.bfloat16), "tp", 0
    ).astype(jnp.bfloat16)


def solution(mesh):
    finer = Mesh(mesh.devices.reshape(8, 8, mesh.shape["tp"]), ("sp_0", "sp_1", "tp"))
    in_specs = (
        P(SP_TP, None),
        P(),
        P(SP, "tp"),
        P(SP, "tp"),
        P(SP, "tp"),
        P(),
        P(None, "tp"),
        P("tp"),
        P(SP),
        P(),
        P("tp", SP),
    )
    out_specs = P(SP_TP, None)
    return jax.shard_map(
        on_device, mesh=finer, in_specs=in_specs, out_specs=out_specs, check_vma=False
    )
```

profile of v0, /device:TPU:1, one launch (start us, length us, event | category | flops | bytes accessed | tf_op | source)
XLA Modules:
  0.0 498.0 jit_solution(9612616746641343713)
XLA Ops:
  7.8 2.0 fusion.61
  12.5 40.7 %all-gather.9.cloned.1.call-done = bf16[1024,2048]{1,0:T(8,128)(2,1)} async-done(((bf16[128,2048]{1,0:T(8,128)(2,1)}), bf16[1024,2048]{1,0:T(8,128)(2,1)}) %all-gather.9.cloned.1.call-update) | async-done | bytes 4194320 | tf_op jit(solution)/shard_map/all_gather | solution.py:149
  53.2 85.4 %all-gather.11.cloned.1.call-done = bf16[2048,1024]{1,0:T(8,128)(2,1)} async-done(((bf16[32,1024]{1,0:T(8,128)(2,1)}), bf16[2048,1024]{1,0:T(8,128)(2,1)}) %all-gather.11.cloned.1.call-update) | async-done | bytes 4194320 | tf_op jit(solution)/shard_map/all_gather | solution.py:18
  138.6 8.1 %fusion.51 = bf16[1024,1040]{0,1:T(8,128)(2,1)S(1)} fusion(bf16[1024,2048]{1,0:T(8,128)(2,1)} %all-gather.9.cloned.1.call-done, bf16[2048,16]{1,0:T(8,128)(2,1)S(1)} %copy.37, bf16[2048,1024]{1,0:T(8,128)(2,1)} %all-gather.11.cloned.1.call-done), kind=kOutput, calls=%fused_computation.62 | convolution fusion | flops 4371660800 | bytes 10584064 | tf_op jit(solution)/shard_map/dot_general | solution.py:148
  148.0 1.9 fusion.64
  149.8 2.5 copy.39
  152.4 3.4 copy.42
  157.3 2.1 copy.43
  160.7 48.5 %while.31 = (s32[]{:T(128)}, f32[1,256,512]{2,1,0:T(8,128)S(1)}, f32[16,1,256]{2,1,0:T(1,128)S(1)}, f32[16,64,1,256]{3,2,1,0:T(1,128)}, f32[16,64,1,256]{3,2,1,0...) while((s32[]{:T(128)}, f32[1,256,512]{2,1,0:T(8,128)S(1)}, ...), condition=%wide.region_3.4_spmd.clone, body=%wide.region_1.3_spmd.clone.sunk | while | flops 18251780 | bytes 1450087 | solution.py:110
  210.2 11.0 %all-gather.2 = f32[8,1,256]{2,1,0:T(1,128)S(1)} all-gather(f32[1,1,256]{2,1,0:T(1,128)S(1)} %bitcast.299), channel_id=2, replica_groups=mesh['sp_0'=8,'sp_1'=8,'tp'=8] {'sp_1'}, dimensions={0}, use_global_device_ids=true | all-gather | bytes 9216 | tf_op jit(solution)/shard_map/all_gather | solution.py:36
  221.2 46.4 %all-gather.17.cloned.1.call-done = f32[8,256,512]{2,1,0:T(8,128)} async-done(((f32[1,256,512]{2,1,0:T(8,128)}), f32[8,256,512]{2,1,0:T(8,128)}) %all-gather.17.cloned.1.call-update) | async-done | bytes 4194320 | tf_op jit(solution)/shard_map/all_gather | solution.py:36
  267.6 3.3 bitcast_add_fusion.1
  271.7 13.7 %all_gather.30 = f32[8,1,256]{2,1,0:T(1,128)S(1)} all-gather(f32[1,1,256]{2,1,0:T(1,128)S(1)} %get-tuple-element.230), channel_id=1, replica_groups=mesh['sp_0'=8,'sp_1'=8,'tp'=8] {'sp_0'}, dimensions={0}, use_global_device_ids=true | all-gather | bytes 9216 | tf_op jit(solution)/shard_map/all_gather | solution.py:36
  285.7 42.6 %all-gather.13.cloned.1.call-done = f32[8,1,256,512]{3,2,1,0:T(8,128)} async-done(((f32[1,1,256,512]{3,2,1,0:T(8,128)}), f32[8,1,256,512]{3,2,1,0:T(8,128)}) %all-gather.13.cloned.1.call-update) | async-done | bytes 4194320 | tf_op jit(solution)/shard_map/all_gather | solution.py:36
  328.3 4.3 fusion.68
  332.6 93.2 %while.30 = (s32[]{:T(128)}, f32[1,256,512]{2,1,0:T(8,128)S(1)}, f32[16,64,1,512]{3,1,2,0:T(8,128)}, bf16[16,64,1,256]{3,1,0,2:T(8,128)(2,1)S(1)}, bf16[16,1,256...) while((s32[]{:T(128)}, f32[1,256,512]{2,1,0:T(8,128)S(1)}, ...), condition=%wide.region_7.8_spmd.clone, body=%wide.region_5.7_spmd.clone.sunk | while | flops 24555520 | bytes 3223153 | solution.py:87
  340.6 1.8 fusion.117
  346.4 1.8 fusion.117
  363.9 1.8 fusion.117
  404.7 1.8 fusion.117
  425.8 3.8 multiply_reduce_fusion
  430.0 4.0 convolution_convert_fusion
  434.0 53.6 %all_to_all.5 = bf16[8,128,2048]{2,1,0:T(8,128)(2,1)} all-to-all(bf16[8,128,2048]{2,1,0:T(8,128)(2,1)S(1)} %bitcast.263), channel_id=1, replica_groups=mesh['sp_0'=8,'sp_1'=8,'tp'=8] {'tp'}, dimensions={0} | all-to-all | bytes 8388608 | tf_op jit(solution)/shard_map/all_to_all | solution.py:53
  487.7 3.8 reduce_sum.42
  (273 shorter events, 143.4 us)
Async XLA Ops:
  6.5 141.4 %copy-start = (bf16[16,256]{1,0:T(8,128)(2,1)S(1)}, bf16[16,256]{1,0:T(8,128)(2,1)}, u32[]{:S(2)}) copy-start(bf16[16,256]{1,0:T(8,128)(2,1)} %param.21) | copy-start | bytes 24580
  6.5 46.7 %all-gather.9.cloned.1.call-start = ((), (), s32[]{:S(2)}) async-start(), calls=%async_computation.1 | async-start | bytes 4718592 | tf_op jit(solution)/shard_map/all_gather | solution.py:149
  9.8 128.8 %all-gather.11.cloned.1.call-start = ((), (), s32[]{:S(2)}) async-start(), calls=%async_computation.2 | async-start | bytes 4259840 | tf_op jit(solution)/shard_map/all_gather | solution.py:18
  11.3 256.3 %all-gather.17.cloned.1.call-start = ((), (), s32[]{:S(2)}) async-start(), calls=%async_computation.5 | async-start | bytes 4718592 | tf_op jit(solution)/shard_map/all_gather | solution.py:36
  12.5 135.5 %copy-start.6 = (f32[1024]{0:T(1024)S(1)}, f32[1024]{0:T(1024)}, u32[]{:S(2)}) copy-start(f32[1024]{0:T(1024)} %param.23) | copy-start | bytes 12292
  12.5 135.4 %copy-start.7 = (f32[256]{0:T(256)S(1)}, f32[256]{0:T(256)}, u32[]{:S(2)}) copy-start(f32[256]{0:T(256)} %param.22) | copy-start | bytes 3076
  146.7 5.6 %copy-start.2 = (bf16[1024,1040]{0,1:T(8,128)(2,1)}, bf16[1024,1040]{0,1:T(8,128)(2,1)S(1)}, u32[]{:S(2)}) copy-start(bf16[1024,1040]{0,1:T(8,128)(2,1)S(1)} %fusion.51) | copy-start | bytes 6389764
  152.4 7.1 %slice-start = ((bf16[1024,1040]{0,1:T(8,128)(2,1)}), bf16[1024,512]{0,1:T(8,128)(2,1)S(1)}, s32[]{:S(2)}) async-start(bf16[1024,1040]{0,1:T(8,128)(2,1)} %copy-done.2), calls=%async_computation.6 | async-start | bytes 2097152 | tf_op jit(solution)/shard_map/slice | solution.py:156
  209.2 0.8 copy-start.1
  209.2 62.3 %copy-start.3 = (bf16[1024,1040]{0,1:T(8,128)(2,1)S(1)}, bf16[1024,1040]{0,1:T(8,128)(2,1)}, u32[]{:S(2)}) copy-start(bf16[1024,1040]{0,1:T(8,128)(2,1)} %copy-done.2) | copy-start | bytes 6389764
  210.0 118.2 %all-gather.13.cloned.1.call-start = ((), (), s32[]{:S(2)}) async-start(), calls=%async_computation.3 | async-start | bytes 4718592 | tf_op jit(solution)/shard_map/all_gather | solution.py:36
  270.9 159.1 %all-gather.15.cloned.1.call-start = ((), (), s32[]{:S(2)}) async-start(), calls=%async_computation.4 | async-start | bytes 2129920 | tf_op jit(solution)/shard_map/all_gather | solution.py:167
  328.3 4.3 copy-start.4
  425.8 3.9 copy-start.5
Sparse Core Ops, SparseCore 0:
  10.0 43.2 all-gather.8
  56.3 82.2 all-gather.10
  210.2 57.3 all-gather.16
  271.0 57.2 all-gather.12
  331.2 77.5 all-gather.14
where the time goes:
time: 504 us; the launch traced here: 498 us
  waiting for transfers between devices  216 us (43%)
  matrix products  82.2 us (16%)
  other arithmetic  81 us (16%)
  blocking collectives  78.3 us (16%)
  local copies, waits for them, and re-layouts  25.8 us (5%)
  between operations  13.4 us (3%)
    all_gather x2, waiting for transfers between devices, entering(): pieces = jax.tree.map(lambda part: lax.all_gather(part, axis), total)  89 us
    all_gather x1, waiting for transfers between devices, sent_together(): lax.all_gather(both, axis, axis=dim, tiled=True)  85.4 us
    all_to_all x1, blocking collectives, sent_and_summed(): parts = lax.all_to_all(cut_along(value, dim, size), axis, 0, 0, tiled=True)  53.6 us
    all_gather x1, waiting for transfers between devices, on_device(): lax.all_gather(normed, 'tp', axis=0, tiled=True)  40.7 us
    dot_general x16, matrix products, local_step(): jnp.einsum('hij,jhe->ihe', scores, v_blk, preferred_element_type=jnp.floa...  28.5 us
    all_gather x2, blocking collectives, entering(): pieces = jax.tree.map(lambda part: lax.all_gather(part, axis), total)  24.7 us
    dot_general x16, matrix products, local_step(): jnp.einsum('jhd,jhe->hde', decayed, v_blk, preferred_element_type=jnp.flo...  18.3 us
    dot_general x16, matrix products, state_step(): jnp.einsum('jhd,jhe->hde', decayed, v_blk, preferred_element_type=jnp.flo...  17.7 us
  transfers between devices with their start and end apart: 5, of which 4 were waited for; matrix products, arithmetic and copies ran while one was open for 21% of the time, Pallas kernels for 0%

commit v1 on v0

--- a/solution.py
+++ b/solution.py
@@ -146,7 +146,9 @@
     heads_here = keys_here // DK
     w_joined = jnp.concatenate([query_w, key_w, value_w, w_rank_down], axis=1)
     joined = jnp.dot(
-        lax.all_gather(normed, "tp", axis=0, tiled=True),
+        jnp.concatenate(
+            lax.all_to_all(jnp.stack([normed] * lax.axis_size("tp")), "tp", 0, 0), axis=0
+        ),
         w_joined,
         preferred_element_type=jnp.float32,
     ).astype(jnp.bfloat16)

time: 504 us -> 464 us (0.921)
  waiting for transfers between devices: 216 us -> 164 us
  starting transfers between devices: 0.17 us -> 11.5 us
    all_gather x1, waiting for transfers between devices: 85.4 us -> 25.4 us  [sent_together(): lax.all_gather(both, axis, axis=dim, tiled=True)]
    all_to_all x0 -> x1, waiting for transfers between devices: none -> 48.5 us  [on_device(): lax.all_to_all(jnp.stack([normed] * lax.axis_size('tp')), 'tp', 0, 0)]
    all_gather x1 -> x0, waiting for transfers between devices: 40.7 us -> none  [on_device(): lax.all_gather(normed, 'tp', axis=0, tiled=True)]
    all_to_all x0 -> x1, starting transfers between devices: none -> 11.4 us  [on_device(): lax.all_to_all(jnp.stack([normed] * lax.axis_size('tp')), 'tp', 0, 0)]
  transfers between devices with their start and end apart: 5 -> 5, of which waited for: 4 -> 4; matrix products, arithmetic and copies ran while one was open for 21% -> 23% of each run, Pallas kernels for 0% -> 0%
where the time goes in v1:
time: 464 us; the launch traced here: 458 us
  waiting for transfers between devices  164 us (35%)
  matrix products  82.2 us (18%)
  other arithmetic  80.2 us (17%)
  blocking collectives  78.3 us (17%)
  local copies, waits for them, and re-layouts  27.5 us (6%)
  between operations  13.4 us (3%)
  starting transfers between devices  11.5 us (2%)
    all_gather x2, waiting for transfers between devices, entering(): pieces = jax.tree.map(lambda part: lax.all_gather(part, axis), total)  89 us
    all_to_all x1, blocking collectives, sent_and_summed(): parts = lax.all_to_all(cut_along(value, dim, size), axis, 0, 0, tiled=True)  53.6 us
    all_to_all x1, waiting for transfers between devices, on_device(): lax.all_to_all(jnp.stack([normed] * lax.axis_size('tp')), 'tp', 0, 0)  48.5 us
    dot_general x16, matrix products, local_step(): jnp.einsum('hij,jhe->ihe', scores, v_blk, preferred_element_type=jnp.floa...  28.5 us
    all_gather x1, waiting for transfers between devices, sent_together(): lax.all_gather(both, axis, axis=dim, tiled=True)  25.4 us
    all_gather x2, blocking collectives, entering(): pieces = jax.tree.map(lambda part: lax.all_gather(part, axis), total)  24.7 us
    dot_general x16, matrix products, local_step(): jnp.einsum('jhd,jhe->hde', decayed, v_blk, preferred_element_type=jnp.flo...  18.3 us
    dot_general x16, matrix products, state_step(): jnp.einsum('jhd,jhe->hde', decayed, v_blk, preferred_element_type=jnp.flo...  17.7 us
  transfers between devices with their start and end apart: 5, of which 4 were waited for; matrix products, arithmetic and copies ran while one was open for 23% of the time, Pallas kernels for 0%

profile of v1, /device:TPU:1, one launch (start us, length us, event | category | flops | bytes accessed | tf_op | source)
XLA Modules:
  0.0 458.0 jit_solution(4430962109284820241)
XLA Ops:
  10.4 2.5 stack.2
  12.9 11.4 %all-to-all-start = ((bf16[8,128,2048]{2,1,0:T(8,128)(2,1)}), bf16[8,128,2048]{2,1,0:T(8,128)(2,1)}, u32[]{:S(2)}, u32[]{:S(2)}) async-start(bf16[8,128,2048]{2,1,0:T(8,128)(2,1)} %stack.2), calls=%async_computation | async-start | bytes 8388608 | tf_op jit(solution)/shard_map/all_to_all | solution.py:150
  24.6 48.5 %all-to-all-done = bf16[8,128,2048]{2,1,0:T(8,128)(2,1)} async-done(((bf16[8,128,2048]{2,1,0:T(8,128)(2,1)}), bf16[8,128,2048]{2,1,0:T(8,128)(2,1)}, u32[]{:S(2)}, u32[]{:S(2)}) %all-to-all-start) | async-done | bytes 4194336 | tf_op jit(solution)/shard_map/all_to_all | solution.py:150
  73.2 25.4 %all-gather.8.cloned.1.call-done = bf16[2048,1024]{1,0:T(8,128)(2,1)} async-done(((bf16[32,1024]{1,0:T(8,128)(2,1)}), bf16[2048,1024]{1,0:T(8,128)(2,1)}) %all-gather.8.cloned.1.call-update) | async-done | bytes 4194320 | tf_op jit(solution)/shard_map/all_gather | solution.py:18
  98.6 8.1 %fusion.51 = bf16[1024,1040]{0,1:T(8,128)(2,1)S(1)} fusion(bf16[1024,2048]{1,0:T(8,128)(2,1)} %bitcast, bf16[2048,16]{1,0:T(8,128)(2,1)S(1)} %copy.37, bf16[2048,1024]{1,0:T(8,128)(2,1)} %all-gather.8.cloned.1.call-done), kind=kOutput, calls=%fused_computation.62 | convolution fusion | flops 4371660800 | bytes 10584064 | tf_op jit(solution)/shard_map/dot_general | solution.py:148
  107.9 1.9 fusion.64
  109.8 2.5 copy.39
  112.3 3.4 copy.42
  117.3 2.1 copy.43
  120.7 48.5 %while.31 = (s32[]{:T(128)}, f32[1,256,512]{2,1,0:T(8,128)S(1)}, f32[16,1,256]{2,1,0:T(1,128)S(1)}, f32[16,64,1,256]{3,2,1,0:T(1,128)}, f32[16,64,1,256]{3,2,1,0...) while((s32[]{:T(128)}, f32[1,256,512]{2,1,0:T(8,128)S(1)}, ...), condition=%wide.region_3.4_spmd.clone, body=%wide.region_1.3_spmd.clone.sunk | while | flops 18251780 | bytes 1450087 | solution.py:110
  170.1 11.0 %all-gather.2 = f32[8,1,256]{2,1,0:T(1,128)S(1)} all-gather(f32[1,1,256]{2,1,0:T(1,128)S(1)} %bitcast.300), channel_id=2, replica_groups=mesh['sp_0'=8,'sp_1'=8,'tp'=8] {'sp_1'}, dimensions={0}, use_global_device_ids=true | all-gather | bytes 9216 | tf_op jit(solution)/shard_map/all_gather | solution.py:36
  181.2 46.4 %all-gather.14.cloned.1.call-done = f32[8,256,512]{2,1,0:T(8,128)} async-done(((f32[1,256,512]{2,1,0:T(8,128)}), f32[8,256,512]{2,1,0:T(8,128)}) %all-gather.14.cloned.1.call-update) | async-done | bytes 4194320 | tf_op jit(solution)/shard_map/all_gather | solution.py:36
  227.6 3.3 bitcast_add_fusion.1
  231.6 13.7 %all_gather.26 = f32[8,1,256]{2,1,0:T(1,128)S(1)} all-gather(f32[1,1,256]{2,1,0:T(1,128)S(1)} %get-tuple-element.230), channel_id=1, replica_groups=mesh['sp_0'=8,'sp_1'=8,'tp'=8] {'sp_0'}, dimensions={0}, use_global_device_ids=true | all-gather | bytes 9216 | tf_op jit(solution)/shard_map/all_gather | solution.py:36
  245.7 42.6 %all-gather.10.cloned.1.call-done = f32[8,1,256,512]{3,2,1,0:T(8,128)} async-done(((f32[1,1,256,512]{3,2,1,0:T(8,128)}), f32[8,1,256,512]{3,2,1,0:T(8,128)}) %all-gather.10.cloned.1.call-update) | async-done | bytes 4194320 | tf_op jit(solution)/shard_map/all_gather | solution.py:36
  288.3 4.3 fusion.68
  292.6 93.2 %while.30 = (s32[]{:T(128)}, f32[1,256,512]{2,1,0:T(8,128)S(1)}, f32[16,64,1,512]{3,1,2,0:T(8,128)}, bf16[16,64,1,256]{3,1,0,2:T(8,128)(2,1)S(1)}, bf16[16,1,256...) while((s32[]{:T(128)}, f32[1,256,512]{2,1,0:T(8,128)S(1)}, ...), condition=%wide.region_7.8_spmd.clone, body=%wide.region_5.7_spmd.clone.sunk | while | flops 24555520 | bytes 3223153 | solution.py:87
  306.4 1.8 fusion.117
  323.9 1.8 fusion.117
  364.6 1.8 fusion.117
  385.8 3.8 multiply_reduce_fusion
  390.0 4.0 convolution_convert_fusion
  394.0 53.6 %all_to_all.10 = bf16[8,128,2048]{2,1,0:T(8,128)(2,1)} all-to-all(bf16[8,128,2048]{2,1,0:T(8,128)(2,1)S(1)} %bitcast.264), channel_id=1, replica_groups=mesh['sp_0'=8,'sp_1'=8,'tp'=8] {'tp'}, dimensions={0} | all-to-all | bytes 8388608 | tf_op jit(solution)/shard_map/all_to_all | solution.py:53
  447.6 3.8 reduce_sum.42
  (275 shorter events, 145.5 us)
Async XLA Ops:
  6.5 101.4 %copy-start = (bf16[16,256]{1,0:T(8,128)(2,1)S(1)}, bf16[16,256]{1,0:T(8,128)(2,1)}, u32[]{:S(2)}) copy-start(bf16[16,256]{1,0:T(8,128)(2,1)} %param.21) | copy-start | bytes 24580
  6.5 92.0 %all-gather.8.cloned.1.call-start = ((), (), s32[]{:S(2)}) async-start(), calls=%async_computation.2 | async-start | bytes 4259840 | tf_op jit(solution)/shard_map/all_gather | solution.py:18
  12.9 11.4 %copy-start.5 = (bf16[2048,16]{0,1:T(8,128)(2,1)S(1)}, bf16[2048,16]{0,1:T(8,128)(2,1)}, u32[]{:S(2)}) copy-start(bf16[2048,16]{0,1:T(8,128)(2,1)} %param.20) | copy-start | bytes 196612
  12.9 60.2 %all-to-all-start = ((bf16[8,128,2048]{2,1,0:T(8,128)(2,1)}), bf16[8,128,2048]{2,1,0:T(8,128)(2,1)}, u32[]{:S(2)}, u32[]{:S(2)}) async-start(bf16[8,128,2048]{2,1,0:T(8,128)(2,1)} %stack.2), calls=%async_computation | async-start | bytes 8388608 | tf_op jit(solution)/shard_map/all_to_all | solution.py:150
  24.3 203.2 %all-gather.14.cloned.1.call-start = ((), (), s32[]{:S(2)}) async-start(), calls=%async_computation.5 | async-start | bytes 4718592 | tf_op jit(solution)/shard_map/all_gather | solution.py:36
  98.6 9.4 %copy-start.7 = (f32[1024]{0:T(1024)S(1)}, f32[1024]{0:T(1024)}, u32[]{:S(2)}) copy-start(f32[1024]{0:T(1024)} %param.23) | copy-start | bytes 12292
  98.6 9.4 %copy-start.8 = (f32[256]{0:T(256)S(1)}, f32[256]{0:T(256)}, u32[]{:S(2)}) copy-start(f32[256]{0:T(256)} %param.22) | copy-start | bytes 3076
  106.7 5.6 %copy-start.2 = (bf16[1024,1040]{0,1:T(8,128)(2,1)}, bf16[1024,1040]{0,1:T(8,128)(2,1)S(1)}, u32[]{:S(2)}) copy-start(bf16[1024,1040]{0,1:T(8,128)(2,1)S(1)} %fusion.51) | copy-start | bytes 6389764
  112.3 7.1 %slice-start = ((bf16[1024,1040]{0,1:T(8,128)(2,1)}), bf16[1024,512]{0,1:T(8,128)(2,1)S(1)}, s32[]{:S(2)}) async-start(bf16[1024,1040]{0,1:T(8,128)(2,1)} %copy-done.2), calls=%async_computation.6 | async-start | bytes 2097152 | tf_op jit(solution)/shard_map/slice | solution.py:158
  169.2 0.8 copy-start.1
  169.2 62.3 %copy-start.3 = (bf16[1024,1040]{0,1:T(8,128)(2,1)S(1)}, bf16[1024,1040]{0,1:T(8,128)(2,1)}, u32[]{:S(2)}) copy-start(bf16[1024,1040]{0,1:T(8,128)(2,1)} %copy-done.2) | copy-start | bytes 6389764
  170.0 118.2 %all-gather.10.cloned.1.call-start = ((), (), s32[]{:S(2)}) async-start(), calls=%async_computation.3 | async-start | bytes 4718592 | tf_op jit(solution)/shard_map/all_gather | solution.py:36
  230.9 159.1 %all-gather.12.cloned.1.call-start = ((), (), s32[]{:S(2)}) async-start(), calls=%async_computation.4 | async-start | bytes 2129920 | tf_op jit(solution)/shard_map/all_gather | solution.py:169
  288.3 4.3 copy-start.4
  385.8 3.9 copy-start.6
Sparse Core Ops, SparseCore 0:
  10.4 88.1 all-gather.7
  170.1 57.3 all-gather.13
  231.0 57.2 all-gather.9
  291.2 77.5 all-gather.11
